TPU v7x, 32 devices: a whole 2x2x4 slice. The times are simulated.
32 devices in a mesh: grp: 2 (over y), sp: 4 (over z), dp: 4 (over x, core).
Axes of the slice: x: 2, y: 2, z: 4, core: 2. Of those that a mesh axis runs over, the one named last changes fastest.
Arguments:
- gate_pre: bfloat16 [8, 1, 1024, 1024], P(('grp', 'dp'), None, 'sp'), parts along dimension 0, may hold values from -6 to 6
- value_pre: bfloat16 [8, 1, 1024, 1024], P(('grp', 'dp'), None, 'sp'), parts along dimension 0, may hold values from -6 to 6
- ln_gain: bfloat16 [1024], replicated, may hold values from 0.099609375 to 1.8984375
- ln_bias: bfloat16 [1024], replicated, may hold values from -3 to 3
- spatial: bfloat16 [8, 1024, 1024], P(None, 'dp'), may hold values from -0.1875 to 0.1875
- spatial_bias: bfloat16 [8, 1024], replicated, may hold values from 0.099609375 to 1.8984375
- out_gain: bfloat16 [1024], replicated, may hold values from 0.099609375 to 1.8984375
- w_out: bfloat16 [1024, 2048], P(None, 'dp'), may hold values from -0.1875 to 0.1875
Outputs:
- mixed_out: bfloat16 [8, 1, 1024, 2048], P(('grp', 'dp'), None, 'sp'), parts along dimension 0
There are 2 independent parts, one for each index of `grp`. A program takes and returns all parts, laid end to end along the dimension named above; an argument that names none is the same for every part. Nothing has to cross between parts.
All inputs are finite; a program needn't handle non-finite values.
Results may differ from a plain program's by a relative error of at most 0.012.
Values may be sent and summed in bfloat16 or wider, within the bound.
A program may use at most 64 MiB of HBM per device.

v0:
```python
import functools

import jax
import jax.numpy as jnp
from jax import lax
from jax.experimental import pallas as pl
from jax.experimental.pallas import tpu as pltpu
from jax.sharding import PartitionSpec as P

HEAD_DIM = 128
SEG = 128


norm_eps = 0.01
gelu_coef = 0.7978845608028654


def gelu_tanh(inputs):
    return (
        0.5 * inputs * (1.0 + jnp.tanh(gelu_coef * (inputs + 0.044715 * inputs * inputs * inputs)))
    )


def on_device(gate_pre, value_pre, ln_gain, ln_bias, spatial, spatial_bias, out_gain, w_out):
    block_total = gate_pre.shape[1]
    share = gate_pre.shape[2]
    feature_count = gate_pre.shape[3]
    token_count = block_total * share
    gate_rows = gate_pre.reshape(token_count, feature_count)
    activated = gelu_tanh(value_pre.reshape(token_count, feature_count).astype(jnp.float32))
    centre = jnp.mean(activated, axis=-1, keepdims=True)
    centered = activated - centre
    variance = jnp.mean(centered * centered, axis=-1, keepdims=True)
    values = (
        centered * lax.rsqrt(variance + norm_eps) * ln_gain.astype(jnp.float32)
        + ln_bias.astype(jnp.float32)
    ).astype(jnp.bfloat16)
    value_cols = lax.all_to_all(values, "sp", split_axis=1, concat_axis=0, tiled=True)
    length = value_cols.shape[0]
    channels = value_cols.shape[1]
    block_len = spatial.shape[2]
    sp_count = lax.axis_size("sp")
    per_head = min(channels, HEAD_DIM)
    head_count = channels // per_head
    first_head = lax.axis_index("sp") * channels // HEAD_DIM
    own_rows = lax.dynamic_slice_in_dim(spatial, first_head, head_count, 0)
    own_bias = lax.dynamic_slice_in_dim(spatial_bias, first_head, head_count, 0)
    arranged = value_cols.reshape(sp_count, block_total, share, head_count, per_head)
    arranged = jnp.transpose(arranged, (3, 0, 2, 1, 4)).reshape(
        head_count, block_len, block_total * per_head
    )
    segment_cols = jnp.arange(block_len) // SEG
    weight_piece = lax.all_gather(own_rows, "dp", axis=1, tiled=True)
    row_count = weight_piece.shape[1]
    segment_rows = jnp.arange(row_count) // SEG
    keep_mask = segment_rows[:, None] >= segment_cols[None, :]
    masked = jnp.where(keep_mask[None], weight_piece, jnp.zeros_like(weight_piece))
    products = jnp.einsum("hij,hjm->him", masked, arranged, preferred_element_type=jnp.float32)
    bias_rows = own_bias.astype(jnp.float32)
    mixed_heads = (products + bias_rows[:, :, None]).astype(jnp.bfloat16)
    mixed_cols = mixed_heads.reshape(head_count, sp_count, share, block_total, per_head)
    mixed_cols = jnp.transpose(mixed_cols, (1, 3, 2, 0, 4)).reshape(length, channels)
    mixed_rows = lax.all_to_all(mixed_cols, "sp", split_axis=0, concat_axis=1, tiled=True)
    gated_rows = gelu_tanh(gate_rows.astype(jnp.float32)) * mixed_rows.astype(jnp.float32)
    scale = lax.rsqrt(jnp.mean(gated_rows * gated_rows, axis=-1, keepdims=True) + norm_eps)
    normed = (gated_rows * scale * out_gain.astype(jnp.float32)).astype(jnp.bfloat16)
    result = jnp.dot(
        normed, lax.all_gather(w_out, "dp", axis=1, tiled=True), preferred_element_type=jnp.float32
    ).astype(jnp.bfloat16)
    return result.reshape(1, block_total, share, result.shape[1])


MESH = pl.DeviceIdType.MESH
CHUNKS = 4
ROWS = 64
VMEM_LIMIT = 67043328


def fused_kernel(
    sp_count,
    gate_hbm, value_hbm, gain_hbm, shift_hbm, spatial, bias_hbm, out_gain_hbm, w_hbm, out_hbm,
    gate_in, value_in, gate_act, vsend, vrecv, msend, mrecv, weights, w_all, normed, out_buf,
    ln_gain, ln_bias, out_gain, bias, total, squares,
    local_sem, out_sem, small_sem,
    v_send, v_recv, m_send, m_recv,
    sx_send, sx_recv, sy_send, sy_recv, sc_send, sc_recv, sf_send, sf_recv, sg_send, sg_recv,
    wx_send, wx_recv, wy_send, wy_recv, wc_send, wc_recv, wf_send, wf_recv, wg_send, wg_recv,
):
    g = lax.axis_index("grp")
    s = lax.axis_index("sp")
    dp = lax.axis_index("dp")
    half = lax.rem(dp, 2)
    core_peer = dp + 1 - 2 * half
    x_peer = lax.rem(dp + 2, 4)
    y_peer = 1 - g
    share, features = value_in.shape
    heads = features // HEAD_DIM
    share_rows = weights.shape[2]
    block_len = weights.shape[3]
    w_cols = w_all.shape[4]
    part_width = gate_act.shape[2]
    first = s * 2

    load_value = pltpu.make_async_copy(value_hbm, value_in, local_sem.at[0])
    load_value.start()
    small = []
    for at, (src, dst) in enumerate(
        ((gain_hbm, ln_gain), (shift_hbm, ln_bias), (bias_hbm, bias), (out_gain_hbm, out_gain))
    ):
        copy = pltpu.make_async_copy(src, dst, small_sem.at[at])
        copy.start()
        small.append(copy)
    load_gate = pltpu.make_async_copy(gate_hbm, gate_in, local_sem.at[1])
    load_gate.start()
    load_spatial = pltpu.make_async_copy(
        spatial.at[pl.ds(first, 2)], weights.at[:, dp], local_sem.at[2]
    )
    load_spatial.start()
    load_w = []
    for part in range(2):
        copy = pltpu.make_async_copy(
            w_hbm.at[:, part], w_all.at[dp, part], local_sem.at[8 + part]
        )
        copy.start()
        load_w.append(copy)

    barrier = pltpu.get_barrier_semaphore()
    for off in range(1, sp_count):
        pl.semaphore_signal(
            barrier, inc=1, device_id={"sp": lax.rem(s + off, sp_count)}, device_id_type=MESH
        )
    pl.semaphore_signal(barrier, inc=1, device_id={"dp": core_peer}, device_id_type=MESH)
    pl.semaphore_signal(barrier, inc=1, device_id={"dp": x_peer}, device_id_type=MESH)
    pl.semaphore_signal(barrier, inc=1, device_id={"grp": y_peer}, device_id_type=MESH)
    pl.semaphore_wait(barrier, sp_count + 2)

    def send(src, dst, ssem, rsem, where):
        copy = pltpu.make_async_remote_copy(
            src_ref=src, dst_ref=dst, send_sem=ssem, recv_sem=rsem,
            device_id=where, device_id_type=MESH,
        )
        return copy

    s_piece = share_rows // CHUNKS

    def s_rows(c):
        return pl.ds(c * s_piece, s_piece)

    sx, wx = [], []
    for c in range(CHUNKS):
        copy = send(
            spatial.at[first + g, s_rows(c)], weights.at[g, dp, s_rows(c)],
            sx_send.at[c], sx_recv.at[c], {"dp": x_peer},
        )
        copy.start()
        sx.append(copy)
    sc = send(
        spatial.at[pl.ds(first, 2)], weights.at[:, dp], sc_send.at[0], sc_recv.at[0],
        {"dp": core_peer},
    )
    sc.start()
    for c in range(sp_count):
        copy = send(
            w_hbm.at[c, g], w_all.at[dp, g, c],
            wx_send.at[c], wx_recv.at[c], {"dp": x_peer},
        )
        copy.start()
        wx.append(copy)

    load_value.wait()
    for copy in small:
        copy.wait()
    gain = ln_gain[...].astype(jnp.float32).reshape(1, features)
    shift = ln_bias[...].astype(jnp.float32).reshape(1, features)

    def normalise(step):
        rows = pl.ds(pl.multiple_of(step * ROWS, ROWS), ROWS)
        activated = gelu_tanh(value_in[rows, :].astype(jnp.float32))
        centre = jnp.mean(activated, axis=-1, keepdims=True)
        centered = activated - centre
        variance = jnp.mean(centered * centered, axis=-1, keepdims=True)
        values = (centered * lax.rsqrt(variance + norm_eps) * gain + shift).astype(jnp.bfloat16)
        for h in range(heads):
            vsend[h, rows, :] = values[:, h * HEAD_DIM : (h + 1) * HEAD_DIM]

    own_rows = pl.ds(pl.multiple_of(s * share, share), share)
    vs = [[], []]

    def send_values(hh, turn, slot, start, size):
        for off in range(1, sp_count):
            there = lax.rem(s + off, sp_count)
            copy = send(
                vsend.at[there * 2 + hh, pl.ds(start, size)],
                vrecv.at[hh, pl.ds(pl.multiple_of(s * share + start, size), size)],
                v_send.at[slot, off - 1], v_recv.at[slot, off - 1], {"sp": there},
            )
            copy.start()
            vs[turn].append(copy)

    for part in range(2):
        pl.loop(part * (share // ROWS // 2), (part + 1) * (share // ROWS // 2))(normalise)
        send_values(g, 0, part, part * (share // 2), share // 2)
    send_values(1 - g, 1, 2, 0, share)
    own_v = []
    for turn in range(2):
        hh = g if turn == 0 else 1 - g
        copy = pltpu.make_async_copy(
            vsend.at[first + hh], vrecv.at[hh, own_rows], local_sem.at[4 + turn]
        )
        copy.start()
        own_v.append(copy)

    def s_forward():
        sy, sf = [], []
        for c in range(CHUNKS):
            sx[c].wait_recv()
            copy = send(
                weights.at[g, x_peer, s_rows(c)], weights.at[g, x_peer, s_rows(c)],
                sy_send.at[c], sy_recv.at[c], {"grp": y_peer},
            )
            copy.start()
            sy.append(copy)
            copy = send(
                weights.at[g, x_peer, s_rows(c)], weights.at[g, x_peer, s_rows(c)],
                sf_send.at[c], sf_recv.at[c], {"dp": core_peer},
            )
            copy.start()
            sf.append(copy)
        return sy, sf

    load_gate.wait()

    @pl.loop(0, share // ROWS)
    def _(step):
        rows = pl.ds(pl.multiple_of(step * ROWS, ROWS), ROWS)
        active = gelu_tanh(gate_in[rows, :].astype(jnp.float32))
        for h in range(heads):
            c = h // 2 * HEAD_DIM
            gate_act[h % 2, rows, c : c + HEAD_DIM] = active[:, h * HEAD_DIM : (h + 1) * HEAD_DIM]

    sy, sf = s_forward()
    for copy in load_w:
        copy.wait()
    wc = send(w_all.at[dp], w_all.at[dp], wc_send.at[0], wc_recv.at[0], {"dp": core_peer})
    wc.start()
    load_spatial.wait()
    sc.wait_recv()

    bias_all = bias[...].astype(jnp.float32)
    head_ids = lax.broadcasted_iota(jnp.int32, bias_all.shape, 0)

    def mix(hh, turn):
        for copy in vs[turn]:
            copy.wait_recv()
        own_v[turn].wait()
        own_bias = jnp.sum(
            jnp.where(head_ids == first + hh, bias_all, 0.0), axis=0, keepdims=True
        )
        for i in range(block_len // SEG):
            k, r = i * SEG // share_rows, i * SEG % share_rows
            reach = (i + 1) * SEG
            term = jnp.transpose(
                jnp.broadcast_to(own_bias[:, i * SEG : (i + 1) * SEG], (HEAD_DIM, SEG))
            )
            product = jnp.dot(
                weights[hh, k, r : r + SEG, :reach], vrecv[hh, :reach, :],
                preferred_element_type=jnp.float32,
            )
            msend[hh, i * SEG : (i + 1) * SEG, :] = (product + term).astype(jnp.bfloat16)
        copies = []
        for off in range(1, sp_count):
            there = lax.rem(s + off, sp_count)
            rows = pl.ds(pl.multiple_of(there * share, share), share)
            copy = send(
                msend.at[hh, rows], mrecv.at[hh, s],
                m_send.at[turn, off - 1], m_recv.at[turn, off - 1], {"sp": there},
            )
            copy.start()
            copies.append(copy)
        copy = pltpu.make_async_copy(
            msend.at[hh, own_rows], mrecv.at[hh, s], local_sem.at[6 + turn]
        )
        copy.start()
        return copies, copy

    for c in range(CHUNKS):
        sf[c].wait_recv()
    m0, own_m0 = mix(g, 0)

    wy, wf, wg = [], [], []

    def w_forward(c):
        wx[c].wait_recv()
        piece = w_all.at[x_peer, g, c]
        copy = send(piece, piece, wy_send.at[c], wy_recv.at[c], {"grp": y_peer})
        copy.start()
        wy.append(copy)
        copy = send(piece, piece, wf_send.at[c], wf_recv.at[c], {"dp": core_peer})
        copy.start()
        wf.append(copy)

    sg = []
    for c in range(CHUNKS):
        if c == 2:
            w_forward(0)
        sy[c].wait_recv()
        piece = weights.at[1 - g, x_peer, s_rows(c)]
        copy = send(piece, piece, sg_send.at[c], sg_recv.at[c], {"dp": core_peer})
        copy.start()
        sg.append(copy)
    for c in range(CHUNKS):
        sg[c].wait_recv()
    m1, own_m1 = mix(1 - g, 1)
    w_forward(1)
    w_forward(2)

    gain_all = out_gain[...].astype(jnp.float32).reshape(1, features)
    gain_parts = [
        jnp.concatenate(
            [gain_all[:, h * HEAD_DIM : (h + 1) * HEAD_DIM] for h in range(part, heads, 2)], axis=1
        )
        for part in range(2)
    ]

    def gate_rows(hh, turn, step):
        rows = pl.ds(pl.multiple_of(step * ROWS, ROWS), ROWS)
        own_gain = jnp.where(hh == 0, gain_parts[0], gain_parts[1])
        mixed = jnp.concatenate([mrecv[hh, c, rows, :] for c in range(sp_count)], axis=-1)
        gated = gate_act[hh, rows, :] * mixed.astype(jnp.float32)
        square = jnp.sum(gated * gated, axis=-1, keepdims=True)
        if turn == 0:
            squares[rows, :] = jnp.broadcast_to(square, (ROWS, HEAD_DIM))
        else:
            mean = (squares[rows, :] + square) / features
            squares[rows, :] = lax.rsqrt(mean + norm_eps)
        normed[hh, rows, :] = (gated * own_gain).astype(jnp.bfloat16)

    def product(hh, k):
        return jnp.dot(
            normed[hh], w_all[k, hh].reshape(part_width, w_cols),
            preferred_element_type=jnp.float32,
        )

    for copy in m0:
        copy.wait_recv()
    own_m0.wait()
    pl.loop(0, share // ROWS)(functools.partial(gate_rows, g, 0))
    order = [dp, core_peer, x_peer, lax.rem(core_peer + 2, 4)]
    total[0] = product(g, order[0])
    wc.wait_recv()
    total[1] = product(g, order[1])
    w_forward(3)
    total[2] = product(g, order[2])
    for copy in wf:
        copy.wait_recv()
    total[3] = product(g, order[3])

    def w_pass(c):
        wy[c].wait_recv()
        piece = w_all.at[x_peer, 1 - g, c]
        copy = send(piece, piece, wg_send.at[c], wg_recv.at[c], {"dp": core_peer})
        copy.start()
        wg.append(copy)

    for c in range(sp_count - 2):
        w_pass(c)
    for copy in m1:
        copy.wait_recv()
    own_m1.wait()
    pl.loop(0, share // ROWS)(functools.partial(gate_rows, 1 - g, 1))

    outs = []
    for at, k in enumerate(order):
        if at == 1:
            w_pass(sp_count - 2)
        if at == 2:
            w_pass(sp_count - 1)
        if at == 3:
            for copy in wg:
                copy.wait_recv()
        summed = (total[at] + product(1 - g, k)) * squares[:, :1]
        out_buf[at] = summed.astype(jnp.bfloat16)
        columns = pl.ds(pl.multiple_of(k * w_cols, w_cols), w_cols)
        copy = pltpu.make_async_copy(out_buf.at[at], out_hbm.at[:, columns], out_sem.at[at])
        copy.start()
        outs.append(copy)

    for copy in sx + [sc] + wx + vs[0] + vs[1] + sy + sf + [wc] + m0 + sg + m1 + wy + wf + wg:
        copy.wait_send()
    for copy in outs:
        copy.wait()


def fused(mesh_shape, gate_pre, value_pre, ln_gain, ln_bias, spatial, spatial_bias, out_gain, w_out):
    share, features = gate_pre.shape[2:]
    dp_count, sp_count = mesh_shape["dp"], mesh_shape["sp"]
    heads, share_rows, block_len = spatial.shape
    w_cols = w_out.shape[1]
    width = w_cols * dp_count
    bf16 = jnp.bfloat16
    dma = pltpu.SemaphoreType.DMA
    any_space = pl.BlockSpec(memory_space=pl.ANY)
    hbm = pl.BlockSpec(memory_space=pltpu.HBM)
    part_width = features // 2
    link_sems = []
    pieces = [CHUNKS, CHUNKS, 1, CHUNKS, CHUNKS]
    w_pieces = [sp_count, sp_count, 1, sp_count, sp_count]
    for count in pieces + w_pieces:
        link_sems += [dma((count,)), dma((count,))]
    others = sp_count - 1
    result = pl.pallas_call(
        functools.partial(fused_kernel, sp_count),
        out_shape=jax.ShapeDtypeStruct((share, width), bf16),
        in_specs=[any_space, any_space, hbm, hbm, any_space, hbm, hbm, any_space],
        out_specs=any_space,
        scratch_shapes=[
            pltpu.VMEM((share, features), bf16),
            pltpu.VMEM((share, features), bf16),
            pltpu.VMEM((2, share, part_width), jnp.float32),
            pltpu.VMEM((heads, share, HEAD_DIM), bf16),
            pltpu.VMEM((2, block_len, HEAD_DIM), bf16),
            pltpu.VMEM((2, block_len, HEAD_DIM), bf16),
            pltpu.VMEM((2, sp_count, share, HEAD_DIM), bf16),
            pltpu.VMEM((2, dp_count, share_rows, block_len), bf16),
            pltpu.VMEM((dp_count, 2, sp_count, HEAD_DIM, w_cols), bf16),
            pltpu.VMEM((2, share, part_width), bf16),
            pltpu.VMEM((dp_count, share, w_cols), bf16),
            pltpu.VMEM((features,), bf16),
            pltpu.VMEM((features,), bf16),
            pltpu.VMEM((features,), bf16),
            pltpu.VMEM((heads, block_len), bf16),
            pltpu.VMEM((dp_count, share, w_cols), jnp.float32),
            pltpu.VMEM((share, HEAD_DIM), jnp.float32),
            dma((10,)),
            dma((dp_count,)),
            dma((4,)),
            dma((3, others)), dma((3, others)), dma((2, others)), dma((2, others)),
        ] + link_sems,
        compiler_params=pltpu.CompilerParams(
            collective_id=0, has_side_effects=True, vmem_limit_bytes=VMEM_LIMIT
        ),
    )(
        gate_pre.reshape(share, features), value_pre.reshape(share, features),
        ln_gain, ln_bias, spatial, spatial_bias, out_gain,
        w_out.reshape(sp_count, 2, HEAD_DIM, w_cols),
    )
    return result.reshape(1, 1, share, width)


def body_for(mesh_shape):
    def body(*arrays):
        gate_pre, spatial = arrays[0], arrays[4]
        blocks, share, features = gate_pre.shape[1:]
        heads, share_rows, block_len = spatial.shape
        fits = (
            mesh_shape["grp"] == 2
            and mesh_shape["dp"] == 4
            and blocks == 1
            and features == heads * HEAD_DIM
            and heads == 2 * mesh_shape["sp"]
            and share % SEG == 0
            and share_rows % SEG == 0
        )
        if fits:
            return fused(mesh_shape, *arrays)
        return on_device(*arrays)

    return body


def solution(mesh):
    in_specs = (
        P(("grp", "dp"), None, "sp", None),
        P(("grp", "dp"), None, "sp", None),
        P(),
        P(),
        P(None, "dp", None),
        P(),
        P(),
        P(None, "dp"),
    )
    out_specs = P(("grp", "dp"), None, "sp", None)
    return jax.shard_map(
        body_for(dict(mesh.shape)), mesh=mesh, in_specs=in_specs, out_specs=out_specs, check_vma=False
    )
```

profile of v0, /device:TPU:0, one launch (start us, length us, event | category | flops | bytes accessed | tf_op | source)
XLA Modules:
  0.0 40.6 jit_solution(10556057129999764160)
XLA Ops:
  0.0 38.2 %shard_map.82 = bf16[256,2048]{1,0:T(8,128)(2,1)} custom-call(bf16[256,1024]{1,0:T(8,128)(2,1)} %bitcast.6, bf16[256,1024]{1,0:T(8,128)(2,1)} %bitcast.7, bf16[1024]{0:T(1024)(128)(2,1)} %gain_hbm.1, bf16[1024]{0:T(1024)(128)(2,1)} %shift_hbm.1, bf16[8,256,1024]{2,1,0:T(8,128)(2,1)} %spatial.1, bf16[8,1024]{1,0:T(8,128)(2,1)} %bias_hbm.1, ...), custom_call_target="tpu_custom_call" | custom-call | tf_op jit(solution)/shard_map/pallas_call | solution.py:411
  38.2 2.3 %copy.10 = bf16[1,1,256,2048]{3,2,1,0:T(8,128)(2,1)} copy(bf16[1,1,256,2048]{3,2,1,0:T(8,128)(2,1)} %bitcast.4) | data formatting | bytes 2097152
where the time goes:
time: 41.3 us; the launch traced here: 40.6 us
  Pallas kernels  38.2 us (92%)
  local copies, waits for them, and re-layouts  2.3 us (6%)
    pallas_call x1, Pallas kernels, fused(): pl.pallas_call(functools.partial(fused_kernel, sp_count), out_shape=jax.S...  38.2 us
    unnamed x1, local copies, waits for them, and re-layouts  2.3 us

commit v1 on v0

v1 whole, which is shorter than its diff:
```python
import functools

import jax
import jax.numpy as jnp
from jax import lax
from jax.experimental import pallas as pl
from jax.experimental.pallas import tpu as pltpu
from jax.sharding import PartitionSpec as P

HEAD_DIM = 128
SEG = 128


norm_eps = 0.01
gelu_coef = 0.7978845608028654


def gelu_tanh(inputs):
    return (
        0.5 * inputs * (1.0 + jnp.tanh(gelu_coef * (inputs + 0.044715 * inputs * inputs * inputs)))
    )


def on_device(gate_pre, value_pre, ln_gain, ln_bias, spatial, spatial_bias, out_gain, w_out):
    block_total = gate_pre.shape[1]
    share = gate_pre.shape[2]
    feature_count = gate_pre.shape[3]
    token_count = block_total * share
    gate_rows = gate_pre.reshape(token_count, feature_count)
    activated = gelu_tanh(value_pre.reshape(token_count, feature_count).astype(jnp.float32))
    centre = jnp.mean(activated, axis=-1, keepdims=True)
    centered = activated - centre
    variance = jnp.mean(centered * centered, axis=-1, keepdims=True)
    values = (
        centered * lax.rsqrt(variance + norm_eps) * ln_gain.astype(jnp.float32)
        + ln_bias.astype(jnp.float32)
    ).astype(jnp.bfloat16)
    value_cols = lax.all_to_all(values, "sp", split_axis=1, concat_axis=0, tiled=True)
    length = value_cols.shape[0]
    channels = value_cols.shape[1]
    block_len = spatial.shape[2]
    sp_count = lax.axis_size("sp")
    per_head = min(channels, HEAD_DIM)
    head_count = channels // per_head
    first_head = lax.axis_index("sp") * channels // HEAD_DIM
    own_rows = lax.dynamic_slice_in_dim(spatial, first_head, head_count, 0)
    own_bias = lax.dynamic_slice_in_dim(spatial_bias, first_head, head_count, 0)
    arranged = value_cols.reshape(sp_count, block_total, share, head_count, per_head)
    arranged = jnp.transpose(arranged, (3, 0, 2, 1, 4)).reshape(
        head_count, block_len, block_total * per_head
    )
    segment_cols = jnp.arange(block_len) // SEG
    weight_piece = lax.all_gather(own_rows, "dp", axis=1, tiled=True)
    row_count = weight_piece.shape[1]
    segment_rows = jnp.arange(row_count) // SEG
    keep_mask = segment_rows[:, None] >= segment_cols[None, :]
    masked = jnp.where(keep_mask[None], weight_piece, jnp.zeros_like(weight_piece))
    products = jnp.einsum("hij,hjm->him", masked, arranged, preferred_element_type=jnp.float32)
    bias_rows = own_bias.astype(jnp.float32)
    mixed_heads = (products + bias_rows[:, :, None]).astype(jnp.bfloat16)
    mixed_cols = mixed_heads.reshape(head_count, sp_count, share, block_total, per_head)
    mixed_cols = jnp.transpose(mixed_cols, (1, 3, 2, 0, 4)).reshape(length, channels)
    mixed_rows = lax.all_to_all(mixed_cols, "sp", split_axis=0, concat_axis=1, tiled=True)
    gated_rows = gelu_tanh(gate_rows.astype(jnp.float32)) * mixed_rows.astype(jnp.float32)
    scale = lax.rsqrt(jnp.mean(gated_rows * gated_rows, axis=-1, keepdims=True) + norm_eps)
    normed = (gated_rows * scale * out_gain.astype(jnp.float32)).astype(jnp.bfloat16)
    result = jnp.dot(
        normed, lax.all_gather(w_out, "dp", axis=1, tiled=True), preferred_element_type=jnp.float32
    ).astype(jnp.bfloat16)
    return result.reshape(1, block_total, share, result.shape[1])


MESH = pl.DeviceIdType.MESH
CHUNKS = 4
ROWS = 64
PIECE = 64
EXTRA = 1
VMEM_LIMIT = 65994752
mark = jax.named_scope


def fused_kernel(
    sp_count,
    gate_hbm, value_hbm, gain_hbm, shift_hbm, spatial, bias_hbm, out_gain_hbm, w_hbm, out,
    gate_in, value_in, gate_act, vsend, vrecv, msend, mrecv, weights, w_all, normed,
    ln_gain, ln_bias, out_gain, bias, total, squares,
    local_sem, small_sem,
    v_send, v_recv, m_send, m_recv,
    sx_send, sx_recv, sy_send, sy_recv, sc_send, sc_recv, sf_send, sf_recv, sg_send, sg_recv,
    wx_send, wx_recv, wy_send, wy_recv, wc_send, wc_recv, wf_send, wf_recv, wg_send, wg_recv,
):
    g = lax.axis_index("grp")
    s = lax.axis_index("sp")
    dp = lax.axis_index("dp")
    half = lax.rem(dp, 2)
    core_peer = dp + 1 - 2 * half
    x_peer = lax.rem(dp + 2, 4)
    y_peer = 1 - g
    share, features = value_in.shape
    heads = features // HEAD_DIM
    dp_count, share_rows, block_len = weights.shape[1:]
    cuts, w_cols = w_all.shape[3], w_all.shape[5]
    pieces = sp_count * cuts
    part_width = gate_act.shape[2]
    relayed = pieces - EXTRA
    first = s * 2

    barrier = pltpu.get_barrier_semaphore()
    for off in range(1, sp_count):
        pl.semaphore_signal(
            barrier, inc=1, device_id={"sp": lax.rem(s + off, sp_count)}, device_id_type=MESH
        )
    pl.semaphore_signal(barrier, inc=1, device_id={"dp": core_peer}, device_id_type=MESH)
    pl.semaphore_signal(barrier, inc=1, device_id={"dp": x_peer}, device_id_type=MESH)
    pl.semaphore_signal(barrier, inc=1, device_id={"grp": y_peer}, device_id_type=MESH)

    load_value = pltpu.make_async_copy(value_hbm, value_in, local_sem.at[0])
    load_value.start()
    small = []
    for at, (src, dst) in enumerate(
        ((gain_hbm, ln_gain), (shift_hbm, ln_bias), (bias_hbm, bias), (out_gain_hbm, out_gain))
    ):
        copy = pltpu.make_async_copy(src, dst, small_sem.at[at])
        copy.start()
        small.append(copy)
    load_gate = pltpu.make_async_copy(gate_hbm, gate_in, local_sem.at[1])
    load_gate.start()
    load_spatial = pltpu.make_async_copy(
        spatial.at[pl.ds(first, 2)], weights.at[:, dp], local_sem.at[2]
    )
    load_spatial.start()
    load_w = []
    for part in range(2):
        copy = pltpu.make_async_copy(
            w_hbm.at[:, part], w_all.at[dp, part], local_sem.at[8 + part]
        )
        copy.start()
        load_w.append(copy)

    def send(src, dst, ssem, rsem, where):
        return pltpu.make_async_remote_copy(
            src_ref=src, dst_ref=dst, send_sem=ssem, recv_sem=rsem,
            device_id=where, device_id_type=MESH,
        )

    def on_dp(action):
        for k in range(dp_count):
            pl.when(dp == k)(functools.partial(action, k))

    s_piece = share_rows // CHUNKS

    def s_part(ref, lead, k, c):
        cols = (k * share_rows + (c + 1) * s_piece + SEG - 1) // SEG * SEG
        return ref.at[(*lead, pl.ds(c * s_piece, s_piece), pl.ds(0, cols))]

    def sx_copy(k, c):
        return send(
            s_part(spatial, (first + g,), k, c), s_part(weights, (g, k), k, c),
            sx_send.at[c], sx_recv.at[c], {"dp": x_peer},
        )

    def relay(head, k, c, ssem, rsem, where):
        piece = s_part(weights, (head, k), k, c)
        return send(piece, piece, ssem.at[c], rsem.at[c], where)

    def sx_in(k, c):
        return relay(g, k, c, sx_send, sx_recv, {"dp": x_peer})

    def sy_copy(k, c):
        return relay(g, k, c, sy_send, sy_recv, {"grp": y_peer})

    def sf_copy(k, c):
        return relay(g, k, c, sf_send, sf_recv, {"dp": core_peer})

    def sy_in(k, c):
        return relay(1 - g, k, c, sy_send, sy_recv, {"grp": y_peer})

    def sg_copy(k, c):
        return relay(1 - g, k, c, sg_send, sg_recv, {"dp": core_peer})

    def w_piece(k, part, p):
        return w_all.at[k, part, p // cuts, p % cuts]

    def wx_copy(at):
        part, p = (g, at) if at < pieces else (1 - g, at - pieces + relayed)
        return send(
            w_hbm.at[p // cuts, part, p % cuts], w_piece(dp, part, p),
            wx_send.at[at], wx_recv.at[at], {"dp": x_peer},
        )

    with mark("load_value"):
        load_value.wait()
        for copy in small:
            copy.wait()
    gain = ln_gain[...].astype(jnp.float32).reshape(1, features)
    shift = ln_bias[...].astype(jnp.float32).reshape(1, features)

    def normalise(step):
        rows = pl.ds(pl.multiple_of(step * ROWS, ROWS), ROWS)
        activated = gelu_tanh(value_in[rows, :].astype(jnp.float32))
        centre = jnp.mean(activated, axis=-1, keepdims=True)
        centered = activated - centre
        variance = jnp.mean(centered * centered, axis=-1, keepdims=True)
        values = (centered * lax.rsqrt(variance + norm_eps) * gain + shift).astype(jnp.bfloat16)
        for h in range(heads):
            vsend[h, rows, :] = values[:, h * HEAD_DIM : (h + 1) * HEAD_DIM]

    own_rows = pl.ds(pl.multiple_of(s * share, share), share)
    vs = [[], []]

    def send_values(hh, turn, slot, start, size):
        for off in range(1, sp_count):
            there = lax.rem(s + off, sp_count)
            copy = send(
                vsend.at[there * 2 + hh, pl.ds(start, size)],
                vrecv.at[hh, pl.ds(pl.multiple_of(s * share + start, size), size)],
                v_send.at[slot, off - 1], v_recv.at[slot, off - 1], {"sp": there},
            )
            copy.start()
            vs[turn].append(copy)

    steps = share // ROWS
    with mark("norm0"):
        pl.loop(0, steps // 2)(normalise)
    with mark("barrier"):
        pl.semaphore_wait(barrier, sp_count + 2)
    send_values(g, 0, 0, 0, share // 2)

    @on_dp
    def _(k):
        for c in range(CHUNKS):
            sx_copy(k, c).start()

    sc = send(
        spatial.at[pl.ds(first, 2)], weights.at[:, dp], sc_send.at[0], sc_recv.at[0],
        {"dp": core_peer},
    )
    sc.start()
    wx = [wx_copy(at) for at in range(pieces + EXTRA)]
    for copy in wx:
        copy.start()
    with mark("norm1"):
        pl.loop(steps // 2, steps)(normalise)
    send_values(g, 0, 1, share // 2, share // 2)
    send_values(1 - g, 1, 2, 0, share)
    own_v = []
    for turn in range(2):
        hh = g if turn == 0 else 1 - g
        copy = pltpu.make_async_copy(
            vsend.at[first + hh], vrecv.at[hh, own_rows], local_sem.at[4 + turn]
        )
        copy.start()
        own_v.append(copy)

    load_gate.wait()

    with mark("gact"):

        @pl.loop(0, steps)
        def _(step):
            rows = pl.ds(pl.multiple_of(step * ROWS, ROWS), ROWS)
            active = gelu_tanh(gate_in[rows, :].astype(jnp.float32))
            for h in range(heads):
                c = h // 2 * HEAD_DIM
                gate_act[h % 2, rows, c : c + HEAD_DIM] = active[
                    :, h * HEAD_DIM : (h + 1) * HEAD_DIM
                ]

    for copy in load_w:
        copy.wait()
    wc = send(w_all.at[dp], w_all.at[dp], wc_send.at[0], wc_recv.at[0], {"dp": core_peer})
    wc.start()

    @on_dp
    def _(k):
        there = (k + 2) % dp_count
        for c in range(CHUNKS):
            with mark(f"sx{c}"):
                sx_in(there, c).wait_recv()
            sy_copy(there, c).start()
            sf_copy(there, c).start()
            if c:
                with mark(f"sy{c - 1}"):
                    sy_in(there, c - 1).wait_recv()
                sg_copy(there, c - 1).start()

    wy, wf, wg = [], [], []

    def w_in(at):
        with mark(f"wx{at}"):
            wx[at].wait_recv()
        part, p = (g, at) if at < pieces else (1 - g, at - pieces + relayed)
        piece = w_piece(x_peer, part, p)
        if at < relayed:
            copy = send(piece, piece, wy_send.at[at], wy_recv.at[at], {"grp": y_peer})
            copy.start()
            wy.append(copy)
        copy = send(piece, piece, wf_send.at[at], wf_recv.at[at], {"dp": core_peer})
        copy.start()
        wf.append(copy)

    def w_pass(at):
        with mark(f"wy{at}"):
            wy[at].wait_recv()
        piece = w_piece(x_peer, 1 - g, at)
        copy = send(piece, piece, wg_send.at[at], wg_recv.at[at], {"dp": core_peer})
        copy.start()
        wg.append(copy)

    bias_all = bias[...].astype(jnp.float32)
    head_ids = lax.broadcasted_iota(jnp.int32, bias_all.shape, 0)

    def m_copy(hh, turn, k):
        rows = pl.ds(k * share, share)
        return send(
            msend.at[hh, rows], mrecv.at[hh, s],
            m_send.at[turn, k], m_recv.at[turn, s], {"sp": k},
        )

    def mix(hh, turn):
        with mark(f"v{turn}"):
            for copy in vs[turn]:
                copy.wait_recv()
            own_v[turn].wait()
        own_bias = jnp.sum(
            jnp.where(head_ids == first + hh, bias_all, 0.0), axis=0, keepdims=True
        )
        low, high = 0, sp_count - 1
        order = []
        while low <= high:
            order += [high, low] if low < high else [low]
            low, high = low + 1, high - 1
        for there in order:
            for i in range(there * share // SEG, (there + 1) * share // SEG):
                k, r = i * SEG // share_rows, i * SEG % share_rows
                reach = (i + 1) * SEG
                term = jnp.transpose(
                    jnp.broadcast_to(own_bias[:, i * SEG : (i + 1) * SEG], (HEAD_DIM, SEG))
                )
                product = jnp.dot(
                    weights[hh, k, r : r + SEG, :reach], vrecv[hh, :reach, :],
                    preferred_element_type=jnp.float32,
                )
                msend[hh, i * SEG : (i + 1) * SEG, :] = (product + term).astype(jnp.bfloat16)
            pl.when(s != there)(lambda there=there: m_copy(hh, turn, there).start())
        copy = pltpu.make_async_copy(
            msend.at[hh, own_rows], mrecv.at[hh, s], local_sem.at[6 + turn]
        )
        copy.start()
        return copy

    def m_arrived(hh, turn):
        for off in range(1, sp_count):
            there = lax.rem(s + off, sp_count)
            send(
                msend.at[hh, own_rows], mrecv.at[hh, there],
                m_send.at[turn, there], m_recv.at[turn, there], {"sp": there},
            ).wait_recv()

    def s_arrived(copy):
        @on_dp
        def _(k):
            there = (k + 1 - 2 * (k % 2) + 2) % dp_count
            for c in range(CHUNKS):
                copy(there, c).wait_recv()

    load_spatial.wait()
    sc.wait_recv()
    w_in(0)
    with mark("sf"):
        s_arrived(sf_copy)
    with mark("mix0"):
        own_m0 = mix(g, 0)
    w_in(1)

    @on_dp
    def _(k):
        there = (k + 2) % dp_count
        with mark("sy3"):
            sy_in(there, CHUNKS - 1).wait_recv()
        sg_copy(there, CHUNKS - 1).start()

    w_in(2)
    with mark("sg"):
        s_arrived(sg_copy)
    with mark("mix1"):
        own_m1 = mix(1 - g, 1)
    w_in(3)
    w_pass(0)
    w_pass(1)
    w_in(4)
    w_pass(2)

    gain_all = out_gain[...].astype(jnp.float32).reshape(1, features)
    gain_parts = [
        jnp.concatenate(
            [gain_all[:, h * HEAD_DIM : (h + 1) * HEAD_DIM] for h in range(part, heads, 2)], axis=1
        )
        for part in range(2)
    ]

    def gate_rows(hh, turn, step):
        rows = pl.ds(pl.multiple_of(step * ROWS, ROWS), ROWS)
        own_gain = jnp.where(hh == 0, gain_parts[0], gain_parts[1])
        mixed = jnp.concatenate([mrecv[hh, c, rows, :] for c in range(sp_count)], axis=-1)
        gated = gate_act[hh, rows, :] * mixed.astype(jnp.float32)
        square = jnp.sum(gated * gated, axis=-1, keepdims=True)
        if turn == 0:
            squares[rows, :] = jnp.broadcast_to(square, (ROWS, HEAD_DIM))
        else:
            mean = (squares[rows, :] + square) / features
            squares[rows, :] = lax.rsqrt(mean + norm_eps)
        normed[hh, rows, :] = (gated * own_gain).astype(jnp.bfloat16)

    def product(hh, k):
        return jnp.dot(
            normed[hh], w_all[k, hh].reshape(part_width, w_cols),
            preferred_element_type=jnp.float32,
        )

    with mark("m0"):
        m_arrived(g, 0)
        own_m0.wait()
    with mark("gate0"):
        pl.loop(0, steps)(functools.partial(gate_rows, g, 0))
    order = [dp, core_peer, x_peer, lax.rem(core_peer + 2, 4)]
    total[0] = product(g, order[0])
    wc.wait_recv()
    total[1] = product(g, order[1])
    w_in(5)
    w_pass(3)
    w_in(6)
    w_pass(4)
    for at in range(7, pieces):
        w_in(at)
    total[2] = product(g, order[2])
    for at in range(5, relayed - 1):
        w_pass(at)
    with mark("wf"):
        for copy in wf[:pieces]:
            copy.wait_recv()
    total[3] = product(g, order[3])
    for at in range(pieces, pieces + EXTRA):
        w_in(at)
    w_pass(relayed - 1)
    with mark("m1"):
        m_arrived(1 - g, 1)
        own_m1.wait()
    with mark("gate1"):
        pl.loop(0, steps)(functools.partial(gate_rows, 1 - g, 1))

    for at, k in enumerate(order):
        if at == 3:
            with mark("wg"):
                for copy in wf[pieces:] + wg:
                    copy.wait_recv()
        summed = (total[at] + product(1 - g, k)) * squares[:, :1]
        columns = pl.ds(pl.multiple_of(k * w_cols, w_cols), w_cols)
        out[:, columns] = summed.astype(jnp.bfloat16)

    with mark("endsend"):

        @on_dp
        def _(k):
            there = (k + 2) % dp_count
            for c in range(CHUNKS):
                sx_copy(k, c).wait_send()
                for copy in (sy_copy, sf_copy, sg_copy):
                    copy(there, c).wait_send()

        for turn, hh in enumerate((g, 1 - g)):
            for off in range(1, sp_count):
                m_copy(hh, turn, lax.rem(s + off, sp_count)).wait_send()
        for copy in [sc] + wx + vs[0] + vs[1] + [wc] + wy + wf + wg:
            copy.wait_send()


def fused(mesh_shape, gate_pre, value_pre, ln_gain, ln_bias, spatial, spatial_bias, out_gain, w_out):
    share, features = gate_pre.shape[2:]
    dp_count, sp_count = mesh_shape["dp"], mesh_shape["sp"]
    heads, share_rows, block_len = spatial.shape
    w_cols = w_out.shape[1]
    width = w_cols * dp_count
    bf16 = jnp.bfloat16
    dma = pltpu.SemaphoreType.DMA
    hbm = pl.BlockSpec(memory_space=pltpu.HBM)
    part_width = features // 2
    pieces = part_width // PIECE
    link_sems = []
    for count in (
        CHUNKS, CHUNKS, 1, CHUNKS, CHUNKS,
        pieces + EXTRA, pieces - EXTRA, 1, pieces + EXTRA, pieces - EXTRA,
    ):
        link_sems += [dma((count,)), dma((count,))]
    others = sp_count - 1
    result = pl.pallas_call(
        functools.partial(fused_kernel, sp_count),
        out_shape=pltpu.VMEM((share, width), bf16),
        in_specs=[hbm] * 8,
        out_specs=pl.BlockSpec(memory_space=pltpu.VMEM),
        scratch_shapes=[
            pltpu.VMEM((share, features), bf16),
            pltpu.VMEM((share, features), bf16),
            pltpu.VMEM((2, share, part_width), jnp.float32),
            pltpu.VMEM((heads, share, HEAD_DIM), bf16),
            pltpu.VMEM((2, block_len, HEAD_DIM), bf16),
            pltpu.VMEM((2, block_len, HEAD_DIM), bf16),
            pltpu.VMEM((2, sp_count, share, HEAD_DIM), bf16),
            pltpu.VMEM((2, dp_count, share_rows, block_len), bf16),
            pltpu.VMEM((dp_count, 2, sp_count, HEAD_DIM // PIECE, PIECE, w_cols), bf16),
            pltpu.VMEM((2, share, part_width), bf16),
            pltpu.VMEM((features,), bf16),
            pltpu.VMEM((features,), bf16),
            pltpu.VMEM((features,), bf16),
            pltpu.VMEM((heads, block_len), bf16),
            pltpu.VMEM((dp_count, share, w_cols), jnp.float32),
            pltpu.VMEM((share, HEAD_DIM), jnp.float32),
            dma((10,)),
            dma((4,)),
            dma((3, others)), dma((3, others)), dma((2, sp_count)), dma((2, sp_count)),
        ] + link_sems,
        compiler_params=pltpu.CompilerParams(
            collective_id=0, has_side_effects=True, vmem_limit_bytes=VMEM_LIMIT
        ),
    )(
        gate_pre.reshape(share, features), value_pre.reshape(share, features),
        ln_gain, ln_bias, spatial, spatial_bias, out_gain,
        w_out.reshape(sp_count, 2, HEAD_DIM // PIECE, PIECE, w_cols),
    )
    return result.reshape(1, 1, share, width)


def body_for(mesh_shape):
    def body(*arrays):
        gate_pre, spatial = arrays[0], arrays[4]
        blocks, share, features = gate_pre.shape[1:]
        heads, share_rows, block_len = spatial.shape
        fits = (
            mesh_shape["grp"] == 2
            and mesh_shape["dp"] == 4
            and blocks == 1
            and features == heads * HEAD_DIM
            and heads == 2 * mesh_shape["sp"]
            and share % SEG == 0
            and share_rows % SEG == 0
        )
        if fits:
            return fused(mesh_shape, *arrays)
        return on_device(*arrays)

    return body


def solution(mesh):
    in_specs = (
        P(("grp", "dp"), None, "sp", None),
        P(("grp", "dp"), None, "sp", None),
        P(),
        P(),
        P(None, "dp", None),
        P(),
        P(),
        P(None, "dp"),
    )
    out_specs = P(("grp", "dp"), None, "sp", None)
    return jax.shard_map(
        body_for(dict(mesh.shape)), mesh=mesh, in_specs=in_specs, out_specs=out_specs, check_vma=False
    )
```

time: 41.3 us -> 36.2 us (0.88); the launches traced: 40.6 us -> 36 us
  Pallas kernels: 38.2 us -> 35.1 us
  local copies, waits for them, and re-layouts: 2.3 us -> 0.97 us
    pallas_call x1, Pallas kernels: 38.2 us -> 35.1 us  [fused(): pl.pallas_call(functools.partial(fused_kernel, sp_count), out_shape=pltpu...]
    unnamed x1, local copies, waits for them, and re-layouts: 2.3 us -> 0.97 us
where the time goes in v1:
time: 36.2 us; the launch traced here: 36 us
  Pallas kernels  35.1 us (97%)
  local copies, waits for them, and re-layouts  0.97 us (3%)
    pallas_call x1, Pallas kernels, fused(): pl.pallas_call(functools.partial(fused_kernel, sp_count), out_shape=pltpu...  35.1 us
    unnamed x1, local copies, waits for them, and re-layouts  0.97 us

profile of v1, /device:TPU:0, one launch (start us, length us, event | category | flops | bytes accessed | tf_op | source)
XLA Modules:
  0.0 36.0 jit_solution(15353516157839863751)
XLA Ops:
  0.0 35.1 %shard_map.82 = bf16[256,2048]{1,0:T(8,128)(2,1)S(1)} custom-call(bf16[256,1024]{1,0:T(8,128)(2,1)} %bitcast.6, bf16[256,1024]{1,0:T(8,128)(2,1)} %bitcast.7, bf16[1024]{0:T(1024)(128)(2,1)} %gain_hbm.1, bf16[1024]{0:T(1024)(128)(2,1)} %shift_hbm.1, bf16[8,256,1024]{2,1,0:T(8,128)(2,1)} %spatial.1, bf16[8,1024]{1,0:T(8,128)(2,1)} %bias_hbm.1, ...), custom_call_target="tpu_custom_call" | custom-call | tf_op jit(solution)/shard_map/pallas_call | solution.py:496
  35.1 1.0 %copy.10 = bf16[1,1,256,2048]{3,2,1,0:T(8,128)(2,1)} copy(bf16[1,1,256,2048]{3,2,1,0:T(8,128)(2,1)S(1)} %bitcast.4) | data formatting | bytes 2097152
